TPU v7x, 32 devices: a whole 2x2x4 slice. The times are simulated.
32 devices in a mesh: grp: 2 (over y), fs: 4 (over z), tp: 4 (over x, core).
Axes of the slice: x: 2, y: 2, z: 4, core: 2. Of those that a mesh axis runs over, the one named last changes fastest.
Arguments:
- tokens: bfloat16 [4096, 2048], P(('grp', 'fs'), 'tp'), parts along dimension 0, may hold values from -36 to 36
- query_matrix: bfloat16 [2048, 1024], P('fs', 'tp'), may hold values from -0.125 to 0.125
- key_weight: bfloat16 [2048, 1024], P('fs', 'tp'), may hold values from -0.125 to 0.125
- value_weight: bfloat16 [2048, 2048], P('fs', 'tp'), may hold values from -0.125 to 0.125
- forget_lower_factor: bfloat16 [2048, 32], replicated, may hold values from -0.125 to 0.125
- decay_up: bfloat16 [32, 1024], replicated, may hold values from -1 to 1
- decay_bias: float32 [1024], replicated, may hold values from -1 to 8
- log_extra: float32 [4096, 1024], P(('grp', 'fs'), 'tp'), parts along dimension 0, may hold values from -0.7 to 0
- head_gain: float32 [256], replicated, may hold values from 0.1 to 1.9
- out_weight: bfloat16 [2048, 2048], P('tp', 'fs'), may hold values from -0.125 to 0.125
- mix_gain: float32 [2048], P('tp'), may hold values from 0.1 to 1.9
- up_weight: bfloat16 [2048, 8192], P('fs', 'tp'), may hold values from -0.125 to 0.125
- down_weight: bfloat16 [8192, 2048], P('tp', 'fs'), may hold values from -0.0625 to 0.0625
- out_gain: float32 [2048], P('tp'), may hold values from 0.1 to 1.9
Outputs:
- layer_out: bfloat16 [4096, 2048], P(('grp', 'fs'), 'tp'), parts along dimension 0
There are 2 independent parts, one for each index of `grp`. A program takes and returns all parts, laid end to end along the dimension named above; an argument that names none is the same for every part. Nothing has to cross between parts.
All inputs are finite; a program needn't handle non-finite values.
Results may differ from a plain program's by a relative error of at most 0.015.
Values may be sent and summed in bfloat16 or wider, within the bound.
A program may use at most 64 MiB of HBM per device.

v0:
```python
import functools

import jax
import jax.numpy as jnp
from jax import lax
from jax.experimental import pallas as pl
from jax.experimental.pallas import tpu as pltpu
from jax.sharding import PartitionSpec as P

DK = 128
DV = 256
CHUNK = 64
SUB = 16
TILE = 256
BAND = 128

ALPHA = 2.0**0.5
TAU = 16.0
EPS = 1e-05

MESH = pl.DeviceIdType.MESH
NT = (((1,), (1,)), ((), ()))
TN = (((0,), (0,)), ((), ()))
BF16, F32 = jnp.bfloat16, jnp.float32


def dot(a, b):
    return jnp.dot(a, b, preferred_element_type=F32)


def loop(count, size, body):
    def step(index, carry):
        body(pl.ds(pl.multiple_of(index * size, size), size))
        return carry

    lax.fori_loop(0, count // size, step, 0)


def when(cond, body):
    if cond is None:
        body()
    else:
        pl.when(cond)(body)


class Sends:
    def __init__(self):
        self.open = []

    def start(self, src, dst, send, recv, device, cond=None):
        def copy():
            return pltpu.make_async_remote_copy(
                src_ref=src, dst_ref=dst, send_sem=send, recv_sem=recv,
                device_id=device, device_id_type=MESH,
            )

        when(cond, lambda: copy().start())
        self.open.append((cond, copy))

    def drain(self):
        for cond, copy in self.open:
            when(cond, lambda copy=copy: copy().wait_send())
        self.open = []


def scan_heads(heads, qkv_ref, decay_ref, gain, out_ref, events):
    rows = qkv_ref.shape[0]
    at_row = lax.broadcasted_iota(jnp.int32, (CHUNK, CHUNK), 0)
    at_col = lax.broadcasted_iota(jnp.int32, (CHUNK, CHUNK), 1)
    tri = (at_row >= at_col).astype(F32)
    sub_row = lax.broadcasted_iota(jnp.int32, (SUB, SUB), 0)
    sub_col = lax.broadcasted_iota(jnp.int32, (SUB, SUB), 1)

    def step(index, states):
        for at, event in events:
            pl.when(index == at)(event)
        here = pl.ds(pl.multiple_of(index * CHUNK, CHUNK), CHUNK)
        fresh_states = []
        for head in range(heads):
            query = qkv_ref[here, head * DK : (head + 1) * DK].astype(F32) * DK**-0.5
            keys = qkv_ref[here, (heads + head) * DK : (heads + head + 1) * DK].astype(F32)
            at_value = 2 * heads * DK + head * DV
            value = qkv_ref[here, at_value : at_value + DV]
            decay = decay_ref[here, head * DK : (head + 1) * DK]
            cumul = jnp.dot(
                tri, decay, precision=lax.Precision.HIGHEST, preferred_element_type=F32
            )
            last = cumul[CHUNK - 1 : CHUNK, :]
            state = states[head]
            out = lax.dot_general(
                (query * jnp.exp(cumul)).astype(BF16),
                state.astype(BF16),
                NT,
                preferred_element_type=F32,
            )
            strips = []
            for a in range(CHUNK // SUB):
                lo, hi = a * SUB, (a + 1) * SUB
                q_a, k_a, g_a = query[lo:hi], keys[lo:hi], cumul[lo:hi]
                diag = jnp.zeros((SUB, SUB), F32)
                for j in range(SUB):
                    weight = jnp.exp(jnp.minimum(g_a - g_a[j : j + 1], 0.0))
                    column = jnp.sum(q_a * k_a[j : j + 1] * weight, axis=1, keepdims=True)
                    diag = jnp.where((sub_col == j) & (sub_row >= j), column, diag)
                strip = dot(diag.astype(BF16), value[lo:hi])
                if a:
                    base = cumul[lo - 1 : lo]
                    before = lax.dot_general(
                        (q_a * jnp.exp(g_a - base)).astype(BF16),
                        (keys[:lo] * jnp.exp(base - cumul[:lo])).astype(BF16),
                        NT,
                        preferred_element_type=F32,
                    )
                    strip += dot(before.astype(BF16), value[:lo])
                strips.append(strip)
            out = out + jnp.concatenate(strips, axis=0)
            fresh = lax.dot_general(
                value,
                (keys * jnp.exp(last - cumul)).astype(BF16),
                TN,
                preferred_element_type=F32,
            )
            fresh_states.append(state * jnp.exp(last) + fresh)
            mean = jnp.mean(out * out, axis=1, keepdims=True)
            out_ref[here, head * DV : (head + 1) * DV] = (
                out * lax.rsqrt(mean + EPS) * gain
            ).astype(BF16)
        return tuple(fresh_states)

    start = tuple(jnp.zeros((DV, DK), F32) for _ in range(heads))
    lax.fori_loop(0, rows // CHUNK, step, start)


def kernel(
    F, T,
    tokens, query, key, value, lower, decay_up, decay_bias, extra, head_gain, out_weight,
    mix_gain, up, down, out_gain,
    result,
    tokg, wqkv, wout, wup, wdown, qkv, decay, mixed, mp, md, xs, xr, mk, v, st, sta, normg, act,
    dnp, dnd, ck, dzs, dzr, dxs, dxr,
    loc, tok_s, tok_r, qz_s, qz_r, qy_s, qy_r, oz_s, oz_r, oy_s, oy_r, uz_s, uz_r, uy_s, uy_r,
    dz_s, dz_r, dy_s, dy_r, md_s, md_r, mx_s, mx_r, st_s, st_r, nm_s, nm_r, dd_s, dd_r,
    dp_s, dp_r, dx_s, dx_r,
):
    U, X = F // T, T // 2
    R, Co = v.shape[1], v.shape[2]
    Rz, W = wqkv.shape[1], wqkv.shape[2]
    kc, vc = query.shape[1], value.shape[1]
    Ko, FH = wout.shape[1], wup.shape[2]
    S = qz_s.shape[2]
    S2 = uz_s.shape[1]
    heads = kc // DK
    g, z, t = lax.axis_index("grp"), lax.axis_index("fs"), lax.axis_index("tp")
    x, c = lax.div(t, 2), lax.rem(t, 2)
    h = lax.rem(z, 2)
    mate = z + 1 - 2 * h
    sends = Sends()

    at_z = lambda other: (g, other, t)
    at_t = lambda other: (g, z, other)
    at_y = (1 - g, z, t)
    at_core = (g, z, t + 1 - 2 * c)
    core = t + 1 - 2 * c

    def arrived(dst, sem, cond=None):
        when(cond, lambda: pltpu.make_async_remote_copy(
            src_ref=dst, dst_ref=dst, send_sem=sem, recv_sem=sem,
            device_id=at_y, device_id_type=MESH,
        ).wait_recv())

    def aligned(value, size):
        return pl.multiple_of(value * size, size)

    copies = [
        pltpu.make_async_copy(query, wqkv.at[z, :, pl.ds(0, kc)], loc.at[0]),
        pltpu.make_async_copy(key, wqkv.at[z, :, pl.ds(kc, kc)], loc.at[1]),
        pltpu.make_async_copy(value, wqkv.at[z, :, pl.ds(2 * kc, vc)], loc.at[2]),
    ]
    tok_copies = [
        pltpu.make_async_copy(tokens.at[:, pl.ds(u * Co, Co)], tokg.at[t * U + u], loc.at[3 + u])
        for u in range(U)
    ]
    late_copies = [
        pltpu.make_async_copy(out_weight, wout.at[z], loc.at[3 + U]),
        pltpu.make_async_copy(up.at[:, pl.ds(aligned(h, FH), FH)], wup.at[z], loc.at[4 + U]),
        pltpu.make_async_copy(down.at[pl.ds(aligned(h, FH), FH), :], wdown.at[z], loc.at[5 + U]),
    ]
    for copy in copies + tok_copies + late_copies:
        copy.start()

    barrier = pltpu.get_barrier_semaphore()
    partners = [at_y]
    partners += [at_z(lax.rem(z + i, F)) for i in range(1, F)]
    partners += [at_t(lax.rem(t + i, T)) for i in range(1, T)]
    for device in partners:
        pl.semaphore_signal(barrier, inc=1, device_id=device, device_id_type=MESH)
    pl.semaphore_wait(barrier, len(partners))

    half = Rz // 2
    step = half // S

    def piece(owner, s, side):
        return wqkv.at[owner, pl.ds(pl.multiple_of(side * half + s * step, step), step), :]

    for copy in copies:
        copy.wait()
    for s in range(S):
        for way, cond in ((0, z < F - 1), (1, z > 0)):
            to = z + 1 - 2 * way
            sends.start(piece(z, s, g), piece(z, s, g), qz_s.at[way, z, s], qz_r.at[z, s], at_z(to), cond)
    for copy in tok_copies:
        copy.wait()
    for i in range(1, T):
        to = lax.rem(t + i, T)
        mine = tokg.at[pl.ds(t * U, U)]
        sends.start(mine, mine, tok_s.at[to], tok_r.at[t], at_t(to))
    for d in range(1, F):
        for s in range(S):
            for way in (0, 1):
                owner = z - d if way == 0 else z + d
                there = z >= d if way == 0 else z + d < F
                onward = (z >= d) & (z < F - 1) if way == 0 else (z + d < F) & (z > 0)
                to = z + 1 - 2 * way
                mine = piece(owner, s, g)
                arrived(mine, qz_r.at[owner, s], there)
                sends.start(mine, mine, qz_s.at[way, owner, s], qz_r.at[owner, s], at_z(to), onward)
                sends.start(mine, mine, qy_s.at[owner, s], qy_r.at[owner, s], at_y, there)

    for copy in late_copies:
        copy.wait()

    def out_piece(owner, side):
        return wout.at[owner, pl.ds(aligned(side, Ko // 2), Ko // 2), :]

    def up_piece(owner, s, side):
        size = Rz // 2 // S2
        return wup.at[owner, pl.ds(pl.multiple_of(side * (Rz // 2) + s * size, size), size), :]

    def down_piece(owner, s, side):
        size = FH // 2 // S2
        return wdown.at[owner, pl.ds(pl.multiple_of(side * (FH // 2) + s * size, size), size), :]

    for i in range(1, F):
        to = lax.rem(z + i, F)
        sends.start(out_piece(z, g), out_piece(z, g), oz_s.at[to], oz_r.at[z], at_z(to))
    for i in range(1, F):
        to = lax.rem(z + i, F)
        part = lax.rem(to, 2)
        size = Rz // 2 // S2
        for s in range(S2):
            rows = pl.ds(pl.multiple_of(g * (Rz // 2) + s * size, size), size)
            sends.start(
                up.at[rows, pl.ds(aligned(part, FH), FH)], up_piece(z, s, g),
                uz_s.at[to, s], uz_r.at[z, s], at_z(to),
            )
    for i in range(1, F):
        to = lax.rem(z + i, F)
        part = lax.rem(to, 2)
        size = FH // 2 // S2
        for s in range(S2):
            rows = pl.ds(pl.multiple_of(part * FH + g * (FH // 2) + s * size, size), size)
            sends.start(
                down.at[rows, :], down_piece(z, s, g), dz_s.at[to, s], dz_r.at[z, s], at_z(to),
            )

    def pass_on(make, z_sem, y_send, y_recv):
        mine = make(g)
        arrived(mine, z_sem)
        sends.start(mine, mine, y_send, y_recv, at_y)

    def out_event(i):
        owner = lax.rem(z + F - i, F)
        mine = out_piece(owner, g)
        here, send, recv = oz_r.at[owner], oy_s.at[owner], oy_r.at[owner]

        def event():
            arrived(mine, here)
            sends.start(mine, mine, send, recv, at_y)

        return event

    def up_event(i, s):
        owner = lax.rem(z + F - i, F)
        pass_on(lambda side: up_piece(owner, s, side), uz_r.at[owner, s], uy_s.at[owner, s], uy_r.at[owner, s])

    def down_event(i, s):
        owner = lax.rem(z + F - i, F)
        pass_on(lambda side: down_piece(owner, s, side), dz_r.at[owner, s], dy_s.at[owner, s], dy_r.at[owner, s])

    for i in range(1, T):
        owner = lax.rem(t + i, T)
        arrived(tokg.at[pl.ds(owner * U, U)], tok_r.at[owner])
    local_up = decay_up[:, pl.ds(aligned(t, kc), kc)]
    local_bias = decay_bias[:, pl.ds(aligned(t, kc), kc)]

    def decay_rows(rows):
        low = dot(tokg[0, rows], lower[0:Co])
        for f in range(1, F):
            low += dot(tokg[f, rows], lower[f * Co : (f + 1) * Co])
        gate = dot(low.astype(BF16), local_up) + local_bias
        logsig = jnp.minimum(gate, 0.0) - jnp.log1p(jnp.exp(-jnp.abs(gate)))
        decay[rows, :] = logsig / TAU + extra[rows, :]

    loop(R, BAND, decay_rows)

    for i in range(1, F):
        owner = lax.rem(z + i, F)
        for s in range(S):
            arrived(piece(owner, s, 1 - g), qy_r.at[owner, s])

    def qkv_columns(cols):
        total = dot(tokg[0], wqkv[0, :, cols])
        for f in range(1, F):
            total += dot(tokg[f], wqkv[f, :, cols])
        qkv[:, cols] = total.astype(BF16)

    loop(W, TILE, qkv_columns)

    chunks = R // CHUNK
    scan_heads(
        heads, qkv, decay, head_gain[...], mixed,
        [(min(chunks - 1, 1 + 2 * i), out_event(i))
         for i in range(1, F)],
    )

    for i in range(1, F):
        owner = lax.rem(z + i, F)
        arrived(out_piece(owner, 1 - g), oy_r.at[owner])
    for i in range(X):
        j = lax.rem(x + 1 + i, X)
        for u in range(U):
            k, block = i * U + u, (2 * j + 1 - c) * U + u

            def other_rows(rows, k=k, block=block):
                mp[k, rows] = dot(mixed[rows], wout[block]).astype(BF16)

            loop(R, TILE, other_rows)
            sends.start(mp.at[k], md.at[k], md_s.at[k], md_r.at[k], at_core)
    for i in range(X):
        j = lax.rem(x + 1 + i, X)
        for u in range(U):
            k, block = i * U + u, (2 * j + c) * U + u
            arrived(md.at[k], md_r.at[k])

            def own_rows(rows, i=i, u=u, k=k, block=block):
                total = dot(mixed[rows], wout[block]) + md[k, rows].astype(F32)
                if i < X - 1:
                    xs[k, rows] = total.astype(BF16)
                else:
                    mk[u, rows] = total

            loop(R, TILE, own_rows)
            if i < X - 1:
                sends.start(xs.at[k], xr.at[x, u], mx_s.at[k], mx_r.at[x, u], at_t(2 * j + c))
    for i in range(1, F):
        for s in range(S2):
            up_event(i, s)

    def share_stats(slot):
        mine = st.at[slot]
        for i in range(1, T):
            to = lax.rem(t + i, T)
            sends.start(mine, sta.at[slot, t], st_s.at[slot, to], st_r.at[slot, t], at_t(to))

    def row_stats(slot, rows, parts):
        ones = jnp.ones((8, Co), F32)
        for kind in range(2):
            total = None
            for part in parts:
                term = lax.dot_general(
                    ones, part * part if kind else part, NT,
                    precision=lax.Precision.HIGHEST, preferred_element_type=F32,
                )
                total = term if total is None else total + term
            st[slot, kind, :, rows] = total
            sta[slot, t, kind, :, rows] = total

    def await_stats(slot):
        for i in range(1, T):
            owner = lax.rem(t + i, T)
            arrived(sta.at[slot, owner], st_r.at[slot, owner])

    def scale_of(slot, rows):
        totals = []
        for kind in range(2):
            total = sta[slot, 0, kind, :, rows]
            for other in range(1, T):
                total += sta[slot, other, kind, :, rows]
            totals.append(total / (Co * F))
        mean = totals[0]
        scale = lax.rsqrt(totals[1] - mean * mean + EPS)
        return mean.T[:, 0:1], scale.T[:, 0:1]

    for i in range(1, X):
        j = lax.rem(x + i, X)
        for u in range(U):
            arrived(xr.at[j, u], mx_r.at[j, u])

    def mix_rows(rows):
        parts = []
        for u in range(U):
            total = mk[u, rows]
            for i in range(1, X):
                total += xr[lax.rem(x + i, X), u, rows].astype(F32)
            total += ALPHA * tokg[t * U + u, rows].astype(F32)
            v[u, rows] = total
            parts.append(total)
        row_stats(0, rows, parts)

    loop(R, BAND, mix_rows)
    share_stats(0)
    await_stats(0)

    def norm_rows(rows):
        mean, scale = scale_of(0, rows)
        for u in range(U):
            gain = mix_gain[:, u * Co : (u + 1) * Co]
            normg[h, t * U + u, rows] = ((v[u, rows] - mean) * scale * gain).astype(BF16)

    loop(R, BAND, norm_rows)

    def region(pair, owner):
        return normg.at[pair, pl.ds(owner * U, U)]

    def forward(pair, owner, slot, device):
        mine = region(pair, owner)
        sends.start(mine, mine, nm_s.at[pair, owner, slot], nm_r.at[pair, owner], device)

    def await_region(pair, owner):
        arrived(region(pair, owner), nm_r.at[pair, owner])

    forward(h, t, X, at_z(mate))
    for i in range(1, X):
        forward(h, t, i, at_t(2 * lax.rem(x + i, X) + c))
    forward(h, t, 0, at_core)
    for i in range(1, X):
        owner = 2 * lax.rem(x + i, X) + c
        await_region(h, owner)
        forward(h, owner, 0, at_core)
    await_region(1 - h, t)
    for i in range(1, X):
        forward(1 - h, t, i, at_t(2 * lax.rem(x + i, X) + c))
    forward(1 - h, t, 0, at_core)
    for i in range(1, F):
        owner = lax.rem(z + i, F)
        for s in range(S2):
            arrived(up_piece(owner, s, 1 - g), uy_r.at[owner, s])

    def hidden(pair):
        for i in range(X):
            await_region(pair, 2 * lax.rem(x + i, X) + 1 - c)

        def hidden_columns(cols):
            total = dot(normg[pair, 0], wup[0, :, cols])
            for f in range(1, F):
                total += dot(normg[pair, f], wup[f, :, cols])
            act[pair, :, cols] = jnp.square(jnp.maximum(total, 0.0)).astype(BF16)

        loop(FH, TILE, hidden_columns)

    hidden(h)
    for i in range(1, X):
        owner = 2 * lax.rem(x + i, X) + c
        await_region(1 - h, owner)
        forward(1 - h, owner, 0, at_core)
    hidden(1 - h)

    for i in range(1, F):
        for s in range(S2):
            down_event(i, s)
    for i in range(1, F):
        owner = lax.rem(z + i, F)
        for s in range(S2):
            arrived(down_piece(owner, s, 1 - g), dy_r.at[owner, s])
    for i in range(X):
        j = lax.rem(x + 1 + i, X)
        for u in range(U):
            k, block = i * U + u, (2 * j + 1 - c) * U + u
            for slot, pair in enumerate((1 - h, h)):

                def other_rows(rows, k=k, block=block, slot=slot, pair=pair):
                    dnp[k, slot, rows] = dot(act[pair, rows], wdown[block]).astype(BF16)

                loop(R, TILE, other_rows)
                sends.start(
                    dnp.at[k, slot], dnd.at[k, slot], dd_s.at[k, slot], dd_r.at[k, slot], at_core
                )
    for i in range(X):
        j = lax.rem(x + 1 + i, X)
        for u in range(U):
            k, block = i * U + u, (2 * j + c) * U + u
            for slot, pair in enumerate((1 - h, h)):
                arrived(dnd.at[k, slot], dd_r.at[k, slot])

                def own_rows(rows, k=k, block=block, slot=slot, pair=pair):
                    total = dot(act[pair, rows], wdown[block]) + dnd[k, slot, rows].astype(F32)
                    if slot == 0:
                        dzs[k, rows] = total.astype(BF16)
                    else:
                        ck[k, rows] = total

                loop(R, TILE, own_rows)
                if slot == 0:
                    sends.start(dzs.at[k], dzr.at[k], dp_s.at[k], dp_r.at[k], at_z(mate))
    for i in range(X):
        j = lax.rem(x + 1 + i, X)
        for u in range(U):
            k = i * U + u
            arrived(dzr.at[k], dp_r.at[k])
            if i < X - 1:

                def pair_rows(rows, k=k):
                    dxs[k, rows] = (ck[k, rows] + dzr[k, rows].astype(F32)).astype(BF16)

                loop(R, BAND, pair_rows)
                sends.start(dxs.at[k], dxr.at[x, u], dx_s.at[k], dx_r.at[x, u], at_t(2 * j + c))
    for i in range(1, X):
        j = lax.rem(x + i, X)
        for u in range(U):
            arrived(dxr.at[j, u], dx_r.at[j, u])

    def last_rows(rows):
        parts = []
        for u in range(U):
            k = (X - 1) * U + u
            total = ck[k, rows] + dzr[k, rows].astype(F32)
            for i in range(1, X):
                total += dxr[lax.rem(x + i, X), u, rows].astype(F32)
            total += ALPHA * normg[h, t * U + u, rows].astype(F32)
            v[u, rows] = total
            parts.append(total)
        row_stats(1, rows, parts)

    loop(R, BAND, last_rows)
    share_stats(1)
    await_stats(1)

    def result_rows(rows):
        mean, scale = scale_of(1, rows)
        for u in range(U):
            gain = out_gain[:, u * Co : (u + 1) * Co]
            result[rows, u * Co : (u + 1) * Co] = ((v[u, rows] - mean) * scale * gain).astype(BF16)

    loop(R, BAND, result_rows)
    sends.drain()


def local(F, T, *args):
    (tokens, query, key, value, lower, decay_up, decay_bias, extra, head_gain, out_weight,
     mix_gain, up, down, out_gain) = args
    U, X = F // T, T // 2
    R, Dt = tokens.shape
    Co = Dt // U
    Rz, kc = query.shape
    W = 2 * kc + value.shape[1]
    Ko = out_weight.shape[0]
    FH = up.shape[1] // 2
    heads = kc // DK
    S, S2 = 2, 2
    vmem, hbm = pl.BlockSpec(memory_space=pltpu.VMEM), pl.BlockSpec(memory_space=pl.ANY)
    sem = lambda *shape: pltpu.SemaphoreType.DMA(shape)
    buf = lambda *shape: pltpu.VMEM(shape, BF16)
    wide = lambda *shape: pltpu.VMEM(shape, F32)
    H = X * U
    scratch = [
        buf(F, R, Co), buf(F, Rz, W), buf(F, Ko, Co), buf(F, Rz, FH), buf(F, FH, Co),
        buf(R, W), wide(R, kc), buf(R, heads * DV),
        buf(H, R, Co), buf(H, R, Co), buf(H, R, Co), buf(X, U, R, Co), wide(U, R, Co),
        wide(U, R, Co), wide(2, 2, 8, R), wide(2, T, 2, 8, R), buf(2, F, R, Co), buf(2, R, FH),
        buf(H, 2, R, Co), buf(H, 2, R, Co), wide(H, R, Co), buf(H, R, Co), buf(H, R, Co),
        buf(H, R, Co), buf(X, U, R, Co),
        sem(6 + U), sem(T), sem(T), sem(2, F, S), sem(F, S), sem(F, S), sem(F, S),
        sem(F), sem(F), sem(F), sem(F),
        sem(F, S2), sem(F, S2), sem(F, S2), sem(F, S2),
        sem(F, S2), sem(F, S2), sem(F, S2), sem(F, S2),
        sem(H), sem(H), sem(H), sem(X, U), sem(2, T), sem(2, T), sem(2, T, X + 1), sem(2, T),
        sem(H, 2), sem(H, 2), sem(H), sem(H), sem(H), sem(X, U),
    ]
    return pl.pallas_call(
        functools.partial(kernel, F, T),
        out_shape=jax.ShapeDtypeStruct((R, Dt), BF16),
        in_specs=[hbm, hbm, hbm, hbm, vmem, vmem, vmem, vmem, vmem, hbm, vmem, hbm, hbm, vmem],
        out_specs=vmem,
        scratch_shapes=scratch,
        compiler_params=pltpu.CompilerParams(
            collective_id=0, has_side_effects=True, vmem_limit_bytes=63 * 2**20
        ),
        name="layer",
    )(
        tokens, query, key, value, lower, decay_up, decay_bias[None], extra, head_gain[None],
        out_weight, mix_gain[None], up, down, out_gain[None],
    )


def solution(mesh):
    in_specs = (
        P(("grp", "fs"), "tp"),
        P("fs", "tp"),
        P("fs", "tp"),
        P("fs", "tp"),
        P(),
        P(),
        P(),
        P(("grp", "fs"), "tp"),
        P(),
        P("tp", "fs"),
        P("tp"),
        P("fs", "tp"),
        P("tp", "fs"),
        P("tp"),
    )
    out_specs = P(("grp", "fs"), "tp")
    body = functools.partial(local, mesh.shape["fs"], mesh.shape["tp"])
    return jax.shard_map(body, mesh=mesh, in_specs=in_specs, out_specs=out_specs, check_vma=False)
```

profile of v0, /device:TPU:0, one launch (start us, length us, event | category | flops | bytes accessed | tf_op | source)
XLA Modules:
  0.0 246.1 jit_solution(17703798335883209106)
XLA Ops:
  0.0 1.9 copy.15.lower
  1.9 242.3 %layer.1 = bf16[512,512]{1,0:T(8,128)(2,1)} custom-call(bf16[512,512]{1,0:T(8,128)(2,1)} %tokens.1, bf16[512,256]{1,0:T(8,128)(2,1)} %query.1, bf16[512,256]{1,0:T(8,128)(2,1)} %key.1, bf16[512,512]{1,0:T(8,128)(2,1)} %value.1, bf16[2048,32]{1,0:T(8,128)(2,1)} %copy.15.lower, bf16[32,1024]{1,0:T(8,128)(2,1)} %decay_up.1, f32[1,1024]{1,0:T(1,128)} %bitcast.4, ...), custom_call_target="tpu_custom_call" | custom-call | tf_op jit(solution)/shard_map/layer/pallas_call | solution.py:579
  244.2 1.9 copy.17
where the time goes:
time: 246 us
  Pallas kernels  242 us (98%)
  local copies, waits for them, and re-layouts  3.78 us (2%)
    pallas_call x1, Pallas kernels, local(): pl.pallas_call(functools.partial(kernel, F, T), out_shape=jax.ShapeDtypeS...  242 us

commit v1 on v0

--- a/solution.py
+++ b/solution.py
@@ -148,7 +148,7 @@
     kc, vc = query.shape[1], value.shape[1]
     Ko, FH = wout.shape[1], wup.shape[2]
     S = qz_s.shape[2]
-    S2 = uz_s.shape[1]
+    S2, S3 = uz_s.shape[1], dz_s.shape[1]
     heads = kc // DK
     g, z, t = lax.axis_index("grp"), lax.axis_index("fs"), lax.axis_index("tp")
     x, c = lax.div(t, 2), lax.rem(t, 2)
@@ -214,21 +214,6 @@
         to = lax.rem(t + i, T)
         mine = tokg.at[pl.ds(t * U, U)]
         sends.start(mine, mine, tok_s.at[to], tok_r.at[t], at_t(to))
-    for d in range(1, F):
-        for s in range(S):
-            for way in (0, 1):
-                owner = z - d if way == 0 else z + d
-                there = z >= d if way == 0 else z + d < F
-                onward = (z >= d) & (z < F - 1) if way == 0 else (z + d < F) & (z > 0)
-                to = z + 1 - 2 * way
-                mine = piece(owner, s, g)
-                arrived(mine, qz_r.at[owner, s], there)
-                sends.start(mine, mine, qz_s.at[way, owner, s], qz_r.at[owner, s], at_z(to), onward)
-                sends.start(mine, mine, qy_s.at[owner, s], qy_r.at[owner, s], at_y, there)
-
-    for copy in late_copies:
-        copy.wait()
-
     def out_piece(owner, side):
         return wout.at[owner, pl.ds(aligned(side, Ko // 2), Ko // 2), :]
 
@@ -236,56 +221,125 @@
         size = Rz // 2 // S2
         return wup.at[owner, pl.ds(pl.multiple_of(side * (Rz // 2) + s * size, size), size), :]
 
+    def columns(s):
+        return pl.ds(s * (Co // S3), Co // S3)
+
     def down_piece(owner, s, side):
-        size = FH // 2 // S2
-        return wdown.at[owner, pl.ds(pl.multiple_of(side * (FH // 2) + s * size, size), size), :]
-
-    for i in range(1, F):
-        to = lax.rem(z + i, F)
-        sends.start(out_piece(z, g), out_piece(z, g), oz_s.at[to], oz_r.at[z], at_z(to))
-    for i in range(1, F):
-        to = lax.rem(z + i, F)
-        part = lax.rem(to, 2)
+        return wdown.at[owner, pl.ds(aligned(side, FH // 2), FH // 2), columns(s)]
+
+    def others(d):
+        return ((z + d, z + d < F), (z - d, z >= d))
+
+    def send_up(d, s, ways=(None, None)):
         size = Rz // 2 // S2
-        for s in range(S2):
-            rows = pl.ds(pl.multiple_of(g * (Rz // 2) + s * size, size), size)
+        rows = pl.ds(pl.multiple_of(g * (Rz // 2) + s * size, size), size)
+        part = lax.rem(h + d, 2)
+        for (to, there), way in zip(others(d), ways):
+            there = there if way is None else there & way
             sends.start(
                 up.at[rows, pl.ds(aligned(part, FH), FH)], up_piece(z, s, g),
-                uz_s.at[to, s], uz_r.at[z, s], at_z(to),
-            )
-    for i in range(1, F):
-        to = lax.rem(z + i, F)
-        part = lax.rem(to, 2)
-        size = FH // 2 // S2
-        for s in range(S2):
-            rows = pl.ds(pl.multiple_of(part * FH + g * (FH // 2) + s * size, size), size)
+                uz_s.at[to, s], uz_r.at[z, s], at_z(to), there,
+            )
+
+    def send_down(d, s, ways=(None, None)):
+        part = lax.rem(h + d, 2)
+        rows = pl.ds(aligned(2 * part + g, FH // 2), FH // 2)
+        for (to, there), way in zip(others(d), ways):
+            there = there if way is None else there & way
             sends.start(
-                down.at[rows, :], down_piece(z, s, g), dz_s.at[to, s], dz_r.at[z, s], at_z(to),
-            )
-
-    def pass_on(make, z_sem, y_send, y_recv):
-        mine = make(g)
-        arrived(mine, z_sem)
-        sends.start(mine, mine, y_send, y_recv, at_y)
-
-    def out_event(i):
-        owner = lax.rem(z + F - i, F)
-        mine = out_piece(owner, g)
-        here, send, recv = oz_r.at[owner], oy_s.at[owner], oy_r.at[owner]
+                down.at[rows, columns(s)], down_piece(z, s, g), dz_s.at[to, s], dz_r.at[z, s], at_z(to),
+                there,
+            )
+
+    def stream(d, mine_of, send, recv, y_send, y_recv, inner_only):
+        for way, (owner, there) in enumerate(((z - d, z >= d), (z + d, z + d < F))):
+            onward = there & ((z < F - 1) if way == 0 else (z > 0))
+            if inner_only:
+                there = onward
+            mine, here = mine_of(owner), recv(owner)
+            arrived(mine, here, there)
+            sends.start(mine, mine, send(way, owner), here, at_z(z + 1 - 2 * way), onward)
+            sends.start(mine, mine, y_send(owner), y_recv(owner), at_y, there)
+
+    def stream_late(d):
+        steps = []
+        for way, (owner, there) in enumerate(((z - d, z >= d), (z + d, z + d < F))):
+            inner = (z < F - 1) if way == 0 else (z > 0)
+            ends = (z == F - 1) if way == 0 else (z == 0)
+            onward = there & inner
+            if d <= F // 2:
+                there, onward = there & ends, None
+            steps.append((
+                out_piece(owner, g), oz_r.at[owner], there, onward, oz_s.at[way, owner],
+                at_z(z + 1 - 2 * way), oy_s.at[owner], oy_r.at[owner],
+            ))
 
         def event():
-            arrived(mine, here)
-            sends.start(mine, mine, send, recv, at_y)
+            for mine, here, there, onward, send, to, y_send, y_recv in steps:
+                arrived(mine, here, there)
+                if onward is not None:
+                    sends.start(mine, mine, send, here, to, onward)
+                sends.start(mine, mine, y_send, y_recv, at_y, there)
 
         return event
 
-    def up_event(i, s):
-        owner = lax.rem(z + F - i, F)
-        pass_on(lambda side: up_piece(owner, s, side), uz_r.at[owner, s], uy_s.at[owner, s], uy_r.at[owner, s])
-
-    def down_event(i, s):
-        owner = lax.rem(z + F - i, F)
-        pass_on(lambda side: down_piece(owner, s, side), dz_r.at[owner, s], dy_s.at[owner, s], dy_r.at[owner, s])
+    def stream_qkv(d, s):
+        stream(
+            d, lambda o: piece(o, s, g), lambda w, o: qz_s.at[w, o, s], lambda o: qz_r.at[o, s],
+            lambda o: qy_s.at[o, s], lambda o: qy_r.at[o, s], False,
+        )
+
+    def stream_out(d):
+        stream(
+            d, lambda o: out_piece(o, g), lambda w, o: oz_s.at[w, o], lambda o: oz_r.at[o],
+            lambda o: oy_s.at[o], lambda o: oy_r.at[o], True,
+        )
+
+    for d in range(1, F):
+        for s in range(S):
+            stream_qkv(d, s)
+        if d == F // 2:
+            late_copies[0].wait()
+            for way, cond in ((0, z < F - 1), (1, z > 0)):
+                mine = out_piece(z, g)
+                sends.start(mine, mine, oz_s.at[way, z], oz_r.at[z], at_z(z + 1 - 2 * way), cond)
+    for d in range(1, F // 2 + 1):
+        stream_out(d)
+    even, odd = h == 0, h == 1
+    for s in range(S2):
+        send_up(1, s)
+        send_up(2, s, (even, odd))
+    for copy in late_copies[1:]:
+        copy.wait()
+
+    def swaps(d, make, z_sem, y_send, y_recv, ways=(None, None)):
+        events = []
+        for (owner, there), way in zip(others(d), ways):
+            there = there if way is None else there & way
+            mine, near, send, recv = make(owner), z_sem(owner), y_send(owner), y_recv(owner)
+
+            def event(mine=mine, near=near, send=send, recv=recv, there=there):
+                arrived(mine, near, there)
+                sends.start(mine, mine, send, recv, at_y, there)
+
+            events.append(event)
+        def run():
+            for event in events:
+                event()
+
+        return run
+
+    def up_swap(d, s):
+        return swaps(
+            d, lambda o: up_piece(o, s, g), lambda o: uz_r.at[o, s], lambda o: uy_s.at[o, s],
+            lambda o: uy_r.at[o, s],
+        )
+
+    def down_swap(d, s, ways=(None, None)):
+        return swaps(
+            d, lambda o: down_piece(o, s, g), lambda o: dz_r.at[o, s], lambda o: dy_s.at[o, s],
+            lambda o: dy_r.at[o, s], ways,
+        )
 
     for i in range(1, T):
         owner = lax.rem(t + i, T)
@@ -294,9 +348,11 @@
     local_bias = decay_bias[:, pl.ds(aligned(t, kc), kc)]
 
     def decay_rows(rows):
-        low = dot(tokg[0, rows], lower[0:Co])
-        for f in range(1, F):
-            low += dot(tokg[f, rows], lower[f * Co : (f + 1) * Co])
+        low = jnp.zeros((BAND, lower.shape[0]), F32)
+        for f in range(F):
+            low += lax.dot_general(
+                tokg[f, rows], lower[:, f * Co : (f + 1) * Co], NT, preferred_element_type=F32
+            )
         gate = dot(low.astype(BF16), local_up) + local_bias
         logsig = jnp.minimum(gate, 0.0) - jnp.log1p(jnp.exp(-jnp.abs(gate)))
         decay[rows, :] = logsig / TAU + extra[rows, :]
@@ -317,12 +373,17 @@
     loop(W, TILE, qkv_columns)
 
     chunks = R // CHUNK
-    scan_heads(
-        heads, qkv, decay, head_gain[...], mixed,
-        [(min(chunks - 1, 1 + 2 * i), out_event(i))
-         for i in range(1, F)],
-    )
-
+    events = []
+    for d in range(1, F):
+        events.append((min(chunks - 1, 2 * d - 1), stream_late(d)))
+    scan_heads(heads, qkv, decay, head_gain[...], mixed, events)
+
+    for s in range(S2):
+        send_up(2, s, (odd, even))
+        for d in range(3, F):
+            send_up(d, s)
+    for s in range(S3):
+        send_down(1, s, (odd, even))
     for i in range(1, F):
         owner = lax.rem(z + i, F)
         arrived(out_piece(owner, 1 - g), oy_r.at[owner])
@@ -352,9 +413,7 @@
             loop(R, TILE, own_rows)
             if i < X - 1:
                 sends.start(xs.at[k], xr.at[x, u], mx_s.at[k], mx_r.at[x, u], at_t(2 * j + c))
-    for i in range(1, F):
-        for s in range(S2):
-            up_event(i, s)
+    up_swap(1, 0)()
 
     def share_stats(slot):
         mine = st.at[slot]
@@ -433,14 +492,31 @@
     for i in range(1, X):
         forward(h, t, i, at_t(2 * lax.rem(x + i, X) + c))
     forward(h, t, 0, at_core)
+    for s in range(S3):
+        send_down(1, s, (even, odd))
+        send_down(2, s, (even, odd))
+    for s in range(1, S2):
+        up_swap(1, s)()
+    for s in range(S2):
+        for d in range(2, F):
+            up_swap(d, s)()
+    await_region(1 - h, t)
+    for s in range(S3):
+        send_down(2, s, (odd, even))
+        for d in range(3, F):
+            send_down(d, s)
+    for i in range(1, X):
+        forward(1 - h, t, i, at_t(2 * lax.rem(x + i, X) + c))
+    forward(1 - h, t, 0, at_core)
+    ends = (z == 0) | (z == F - 1)
+    inside = (z > 0) & (z < F - 1)
+    for s in range(S3):
+        down_swap(1, s, (odd, even))()
+        down_swap(1, s, (even & ends, odd & ends))()
     for i in range(1, X):
         owner = 2 * lax.rem(x + i, X) + c
         await_region(h, owner)
         forward(h, owner, 0, at_core)
-    await_region(1 - h, t)
-    for i in range(1, X):
-        forward(1 - h, t, i, at_t(2 * lax.rem(x + i, X) + c))
-    forward(1 - h, t, 0, at_core)
     for i in range(1, F):
         owner = lax.rem(z + i, F)
         for s in range(S2):
@@ -459,71 +535,91 @@
         loop(FH, TILE, hidden_columns)
 
     hidden(h)
+    for s in range(S3):
+        down_swap(1, s, (even & inside, odd & inside))()
     for i in range(1, X):
         owner = 2 * lax.rem(x + i, X) + c
         await_region(1 - h, owner)
         forward(1 - h, owner, 0, at_core)
+    late = [(d, s) for s in range(S3) for d in range(2, F)]
     hidden(1 - h)
 
-    for i in range(1, F):
-        for s in range(S2):
-            down_event(i, s)
-    for i in range(1, F):
-        owner = lax.rem(z + i, F)
-        for s in range(S2):
-            arrived(down_piece(owner, s, 1 - g), dy_r.at[owner, s])
+    pair_of = lax.div(z, 2)
+    bands = [pl.ds(r * BAND, BAND) for r in range(R // BAND)]
+
+    def await_down(block, s):
+        arrived(down_piece(block, s, 1 - g), dy_r.at[block, s], block != z)
+
+    def project(i, j, u, s):
+        k, cols = i * U + u, columns(s)
+        block = (2 * j + 1 - c) * U + u
+        for slot, pair in enumerate((1 - h, h)):
+
+            def other_rows(rows, block=block, slot=slot, pair=pair):
+                dnp[k, slot, rows, cols] = dot(act[pair, rows], wdown[block, :, cols]).astype(BF16)
+
+            loop(R, TILE, other_rows)
+            mine = (k, slot, slice(None), cols)
+            sends.start(
+                dnp.at[mine], dnd.at[mine], dd_s.at[k, slot, s], dd_r.at[k, slot, s], at_core
+            )
+        block = (2 * j + c) * U + u
+        arrived(dnd.at[k, 0, :, cols], dd_r.at[k, 0, s])
+        for r, rows in enumerate(bands):
+            total = dot(act[1 - h, rows], wdown[block, :, cols])
+            dzs[k, rows, cols] = (total + dnd[k, 0, rows, cols].astype(F32)).astype(BF16)
+            sends.start(
+                dzs.at[k, rows, cols], dzr.at[k, rows, cols], dp_s.at[k, r, s], dp_r.at[k, r, s],
+                at_z(mate),
+            )
+        arrived(dnd.at[k, 1, :, cols], dd_r.at[k, 1, s])
+
+        def own_rows(rows, block=block):
+            total = dot(act[h, rows], wdown[block, :, cols])
+            ck[k, rows, cols] = total + dnd[k, 1, rows, cols].astype(F32)
+
+        loop(R, TILE, own_rows)
+
+    def add_pair(i, j, u, s):
+        k, cols = i * U + u, columns(s)
+        for r, rows in enumerate(bands):
+            arrived(dzr.at[k, rows, cols], dp_r.at[k, r, s])
+            total = ck[k, rows, cols] + dzr[k, rows, cols].astype(F32)
+            dxs[k, rows, cols] = total.astype(BF16)
+            sends.start(
+                dxs.at[k, rows, cols], dxr.at[x, u, rows, cols], dx_s.at[k, r, s],
+                dx_r.at[x, u, r, s], at_t(2 * j + c), j != x,
+            )
+
+    if U > 1:
+        for s in range(S3):
+            for d in range(2, F):
+                down_swap(d, s)()
     for i in range(X):
-        j = lax.rem(x + 1 + i, X)
-        for u in range(U):
-            k, block = i * U + u, (2 * j + 1 - c) * U + u
-            for slot, pair in enumerate((1 - h, h)):
-
-                def other_rows(rows, k=k, block=block, slot=slot, pair=pair):
-                    dnp[k, slot, rows] = dot(act[pair, rows], wdown[block]).astype(BF16)
-
-                loop(R, TILE, other_rows)
-                sends.start(
-                    dnp.at[k, slot], dnd.at[k, slot], dd_s.at[k, slot], dd_r.at[k, slot], at_core
-                )
-    for i in range(X):
-        j = lax.rem(x + 1 + i, X)
-        for u in range(U):
-            k, block = i * U + u, (2 * j + c) * U + u
-            for slot, pair in enumerate((1 - h, h)):
-                arrived(dnd.at[k, slot], dd_r.at[k, slot])
-
-                def own_rows(rows, k=k, block=block, slot=slot, pair=pair):
-                    total = dot(act[pair, rows], wdown[block]) + dnd[k, slot, rows].astype(F32)
-                    if slot == 0:
-                        dzs[k, rows] = total.astype(BF16)
-                    else:
-                        ck[k, rows] = total
-
-                loop(R, TILE, own_rows)
-                if slot == 0:
-                    sends.start(dzs.at[k], dzr.at[k], dp_s.at[k], dp_r.at[k], at_z(mate))
-    for i in range(X):
-        j = lax.rem(x + 1 + i, X)
-        for u in range(U):
-            k = i * U + u
-            arrived(dzr.at[k], dp_r.at[k])
-            if i < X - 1:
-
-                def pair_rows(rows, k=k):
-                    dxs[k, rows] = (ck[k, rows] + dzr[k, rows].astype(F32)).astype(BF16)
-
-                loop(R, BAND, pair_rows)
-                sends.start(dxs.at[k], dxr.at[x, u], dx_s.at[k], dx_r.at[x, u], at_t(2 * j + c))
+        j = lax.rem(pair_of + i, X)
+        for s in range(S3):
+            for block in range(2 * U):
+                await_down(2 * j * U + block, s)
+            for u in range(U):
+                project(i, j, u, s)
+            if i == 0 and U == 1:
+                for d in range(2, F):
+                    down_swap(d, s)()
+        for s in range(S3):
+            for u in range(U):
+                add_pair(i, j, u, s)
     for i in range(1, X):
         j = lax.rem(x + i, X)
         for u in range(U):
-            arrived(dxr.at[j, u], dx_r.at[j, u])
+            for s in range(S3):
+                for r, rows in enumerate(bands):
+                    arrived(dxr.at[j, u, rows, columns(s)], dx_r.at[j, u, r, s])
+    own = lax.rem(x - lax.rem(pair_of, X) + X, X) * U
 
     def last_rows(rows):
         parts = []
         for u in range(U):
-            k = (X - 1) * U + u
-            total = ck[k, rows] + dzr[k, rows].astype(F32)
+            total = ck[own + u, rows] + dzr[own + u, rows].astype(F32)
             for i in range(1, X):
                 total += dxr[lax.rem(x + i, X), u, rows].astype(F32)
             total += ALPHA * normg[h, t * U + u, rows].astype(F32)
@@ -556,7 +652,7 @@
     Ko = out_weight.shape[0]
     FH = up.shape[1] // 2
     heads = kc // DK
-    S, S2 = 2, 2
+    S, S2, S3 = 2, 2, 2 if Co % (2 * DK) == 0 else 1
     vmem, hbm = pl.BlockSpec(memory_space=pltpu.VMEM), pl.BlockSpec(memory_space=pl.ANY)
     sem = lambda *shape: pltpu.SemaphoreType.DMA(shape)
     buf = lambda *shape: pltpu.VMEM(shape, BF16)
@@ -570,11 +666,12 @@
         buf(H, 2, R, Co), buf(H, 2, R, Co), wide(H, R, Co), buf(H, R, Co), buf(H, R, Co),
         buf(H, R, Co), buf(X, U, R, Co),
         sem(6 + U), sem(T), sem(T), sem(2, F, S), sem(F, S), sem(F, S), sem(F, S),
-        sem(F), sem(F), sem(F), sem(F),
+        sem(2, F), sem(F), sem(F), sem(F),
         sem(F, S2), sem(F, S2), sem(F, S2), sem(F, S2),
-        sem(F, S2), sem(F, S2), sem(F, S2), sem(F, S2),
+        sem(F, S3), sem(F, S3), sem(F, S3), sem(F, S3),
         sem(H), sem(H), sem(H), sem(X, U), sem(2, T), sem(2, T), sem(2, T, X + 1), sem(2, T),
-        sem(H, 2), sem(H, 2), sem(H), sem(H), sem(H), sem(X, U),
+        sem(H, 2, S3), sem(H, 2, S3), sem(H, R // BAND, S3), sem(H, R // BAND, S3),
+        sem(H, R // BAND, S3), sem(X, U, R // BAND, S3),
     ]
     return pl.pallas_call(
         functools.partial(kernel, F, T),
@@ -587,7 +684,7 @@
         ),
         name="layer",
     )(
-        tokens, query, key, value, lower, decay_up, decay_bias[None], extra, head_gain[None],
+        tokens, query, key, value, lower.T, decay_up, decay_bias[None], extra, head_gain[None],
         out_weight, mix_gain[None], up, down, out_gain[None],
     )
 

time: 246 us -> 190 us (0.77)
  Pallas kernels: 242 us -> 188 us
    pallas_call x1, Pallas kernels: 242 us -> 188 us  [local(): pl.pallas_call(functools.partial(kernel, F, T), out_shape=jax.ShapeDtypeS...]
where the time goes in v1:
time: 190 us
  Pallas kernels  188 us (99%)
    pallas_call x1, Pallas kernels, local(): pl.pallas_call(functools.partial(kernel, F, T), out_shape=jax.ShapeDtypeS...  188 us

profile of v1, /device:TPU:0, one launch (start us, length us, event | category | flops | bytes accessed | tf_op | source)
XLA Modules:
  0.0 190.0 jit_solution(7572766824736790140)
XLA Ops:
  0.0 188.1 %layer.1 = bf16[512,512]{1,0:T(8,128)(2,1)} custom-call(bf16[512,512]{1,0:T(8,128)(2,1)} %tokens.1, bf16[512,256]{1,0:T(8,128)(2,1)} %query.1, bf16[512,256]{1,0:T(8,128)(2,1)} %key.1, bf16[512,512]{1,0:T(8,128)(2,1)} %value.1, bf16[32,2048]{1,0:T(8,128)(2,1)} %bitcast.5, bf16[32,1024]{1,0:T(8,128)(2,1)} %decay_up.1, f32[1,1024]{1,0:T(1,128)} %bitcast.6, ...), custom_call_target="tpu_custom_call" | custom-call | tf_op jit(solution)/shard_map/layer/pallas_call | solution.py:676
  188.1 1.9 copy.16

commit v2 on v1

--- a/solution.py
+++ b/solution.py
@@ -501,18 +501,23 @@
         for d in range(2, F):
             up_swap(d, s)()
     await_region(1 - h, t)
-    for s in range(S3):
-        send_down(2, s, (odd, even))
-        for d in range(3, F):
-            send_down(d, s)
     for i in range(1, X):
         forward(1 - h, t, i, at_t(2 * lax.rem(x + i, X) + c))
     forward(1 - h, t, 0, at_core)
     ends = (z == 0) | (z == F - 1)
     inside = (z > 0) & (z < F - 1)
+
+    def send_far(only):
+        for s in range(S3):
+            send_down(2, s, (odd & only, even & only))
+            for d in range(3, F):
+                send_down(d, s, (only, only))
+
     for s in range(S3):
         down_swap(1, s, (odd, even))()
         down_swap(1, s, (even & ends, odd & ends))()
+        if s == 0:
+            send_far(ends)
     for i in range(1, X):
         owner = 2 * lax.rem(x + i, X) + c
         await_region(h, owner)
@@ -534,6 +539,7 @@
 
         loop(FH, TILE, hidden_columns)
 
+    send_far(inside)
     hidden(h)
     for s in range(S3):
         down_swap(1, s, (even & inside, odd & inside))()
@@ -543,6 +549,9 @@
         forward(1 - h, owner, 0, at_core)
     late = [(d, s) for s in range(S3) for d in range(2, F)]
     hidden(1 - h)
+    if U == 1:
+        for d in range(2, F):
+            down_swap(d, 0)()
 
     pair_of = lax.div(z, 2)
     bands = [pl.ds(r * BAND, BAND) for r in range(R // BAND)]
@@ -602,12 +611,19 @@
                 await_down(2 * j * U + block, s)
             for u in range(U):
                 project(i, j, u, s)
-            if i == 0 and U == 1:
+            if i == 0 and U == 1 and s > 0:
                 for d in range(2, F):
                     down_swap(d, s)()
-        for s in range(S3):
-            for u in range(U):
-                add_pair(i, j, u, s)
+            if i > 0 and s == 0:
+                for part in range(S3):
+                    for u in range(U):
+                        add_pair(i - 1, lax.rem(pair_of + i - 1, X), u, part)
+            if i == X - 1 and s < S3 - 1:
+                for u in range(U):
+                    add_pair(i, j, u, s)
+    j = lax.rem(pair_of + X - 1, X)
+    for u in range(U):
+        add_pair(X - 1, j, u, S3 - 1)
     for i in range(1, X):
         j = lax.rem(x + i, X)
         for u in range(U):

time: 190 us -> 185 us (0.974)
  Pallas kernels: 188 us -> 183 us
    pallas_call x1, Pallas kernels: 188 us -> 183 us  [local(): pl.pallas_call(functools.partial(kernel, F, T), out_shape=jax.ShapeDtypeS...]
where the time goes in v2:
time: 185 us
  Pallas kernels  183 us (99%)
  local copies, waits for them, and re-layouts  1.87 us (1%)
    pallas_call x1, Pallas kernels, local(): pl.pallas_call(functools.partial(kernel, F, T), out_shape=jax.ShapeDtypeS...  183 us

profile of v2, /device:TPU:0, one launch (start us, length us, event | category | flops | bytes accessed | tf_op | source)
XLA Modules:
  0.0 184.8 jit_solution(14520175284579581494)
XLA Ops:
  0.0 182.9 %layer.1 = bf16[512,512]{1,0:T(8,128)(2,1)} custom-call(bf16[512,512]{1,0:T(8,128)(2,1)} %tokens.1, bf16[512,256]{1,0:T(8,128)(2,1)} %query.1, bf16[512,256]{1,0:T(8,128)(2,1)} %key.1, bf16[512,512]{1,0:T(8,128)(2,1)} %value.1, bf16[32,2048]{1,0:T(8,128)(2,1)} %bitcast.5, bf16[32,1024]{1,0:T(8,128)(2,1)} %decay_up.1, f32[1,1024]{1,0:T(1,128)} %bitcast.6, ...), custom_call_target="tpu_custom_call" | custom-call | tf_op jit(solution)/shard_map/layer/pallas_call | solution.py:692
  182.9 1.9 %copy.16 = bf16[512,512]{1,0:T(8,128)(2,1)} copy(bf16[512,512]{1,0:T(8,128)(2,1)} %layer.1) | data formatting | bytes 1048576

commit v3 on v2

--- a/solution.py
+++ b/solution.py
@@ -624,12 +624,6 @@
     j = lax.rem(pair_of + X - 1, X)
     for u in range(U):
         add_pair(X - 1, j, u, S3 - 1)
-    for i in range(1, X):
-        j = lax.rem(x + i, X)
-        for u in range(U):
-            for s in range(S3):
-                for r, rows in enumerate(bands):
-                    arrived(dxr.at[j, u, rows, columns(s)], dx_r.at[j, u, r, s])
     own = lax.rem(x - lax.rem(pair_of, X) + X, X) * U
 
     def last_rows(rows):
@@ -643,7 +637,13 @@
             parts.append(total)
         row_stats(1, rows, parts)
 
-    loop(R, BAND, last_rows)
+    for r, rows in enumerate(bands):
+        for i in range(1, X):
+            j = lax.rem(x + i, X)
+            for u in range(U):
+                for s in range(S3):
+                    arrived(dxr.at[j, u, rows, columns(s)], dx_r.at[j, u, r, s])
+        last_rows(rows)
     share_stats(1)
     await_stats(1)
 

time: 185 us -> 183 us (0.989)
  Pallas kernels: 183 us -> 181 us
where the time goes in v3:
time: 183 us
  Pallas kernels  181 us (99%)
  local copies, waits for them, and re-layouts  1.87 us (1%)
    pallas_call x1, Pallas kernels, local(): pl.pallas_call(functools.partial(kernel, F, T), out_shape=jax.ShapeDtypeS...  181 us

profile of v3, /device:TPU:0, one launch (start us, length us, event | category | flops | bytes accessed | tf_op | source)
XLA Modules:
  0.0 183.1 jit_solution(9057408027726290841)
XLA Ops:
  0.0 181.2 %layer.1 = bf16[512,512]{1,0:T(8,128)(2,1)} custom-call(bf16[512,512]{1,0:T(8,128)(2,1)} %tokens.1, bf16[512,256]{1,0:T(8,128)(2,1)} %query.1, bf16[512,256]{1,0:T(8,128)(2,1)} %key.1, bf16[512,512]{1,0:T(8,128)(2,1)} %value.1, bf16[32,2048]{1,0:T(8,128)(2,1)} %bitcast.5, bf16[32,1024]{1,0:T(8,128)(2,1)} %decay_up.1, f32[1,1024]{1,0:T(1,128)} %bitcast.6, ...), custom_call_target="tpu_custom_call" | custom-call | tf_op jit(solution)/shard_map/layer/pallas_call | solution.py:692
  181.2 1.9 %copy.16 = bf16[512,512]{1,0:T(8,128)(2,1)} copy(bf16[512,512]{1,0:T(8,128)(2,1)} %layer.1) | data formatting | bytes 1048576
